TPU v7x, 32 devices: a whole 2x2x4 slice. The times are simulated.
32 devices in a mesh: grp: 2 (over y), ep: 4 (over z), tp: 4 (over x, core).
Axes of the slice: x: 2, y: 2, z: 4, core: 2. Of those that a mesh axis runs over, the one named last changes fastest.
Arguments:
- queries: bfloat16 [3072, 1024], P(('grp', 'ep'), 'tp'), parts along dimension 0, may hold values from -6 to 6
- key_values: bfloat16 [3072, 512], P(('grp', 'ep'), 'tp'), parts along dimension 0, may hold values from -6 to 6
- query_gain: float32 [64], replicated, may hold values from 0.5 to 5
- key_gain: float32 [64], replicated, may hold values from 0.5 to 5
- out_weight: bfloat16 [1024, 2048], P('tp'), may hold values from -0.1875 to 0.1875
- second_batch: bfloat16 [4096, 2048], P(('grp', 'ep', 'tp')), parts along dimension 0, may hold values from -6 to 6
- norm_gain: float32 [2048], replicated, may hold values from 0.1 to 1.9
- routes: int32 [4096, 2], P(('grp', 'ep', 'tp')), parts along dimension 0, may hold values from 0 to 7, all different within a row; in each aligned block of 128 rows (0 to 127, 128 to 255, ...) at most 48 rows name the same one
- route_weights: float32 [4096, 2], P(('grp', 'ep', 'tp')), parts along dimension 0, may hold values from 0.2 to 1
- expert_gate: bfloat16 [8, 2048, 1024], P('ep', None, 'tp'), may hold values from -0.125 to 0.125
- expert_up: bfloat16 [8, 2048, 1024], P('ep', None, 'tp'), may hold values from -0.125 to 0.125
- expert_down: bfloat16 [8, 1024, 2048], P('ep', 'tp'), may hold values from -0.1875 to 0.1875
- shared_gate: bfloat16 [2048, 512], P(None, 'tp'), may hold values from -0.125 to 0.125
- shared_up: bfloat16 [2048, 512], P(None, 'tp'), may hold values from -0.125 to 0.125
- shared_down: bfloat16 [512, 2048], P('tp'), may hold values from -0.25 to 0.25
Outputs:
- mixer_out: bfloat16 [3072, 2048], P(('grp', 'ep', 'tp')), parts along dimension 0
- channel_out: bfloat16 [4096, 2048], P(('grp', 'ep', 'tp')), parts along dimension 0
There are 2 independent parts, one for each index of `grp`. A program takes and returns all parts, laid end to end along the dimension named above; an argument that names none is the same for every part. Nothing has to cross between parts.
Inputs may be any that keep to these rules, and one draw needn't show every extreme that they name: `routes`: each row names 2 different experts. Among the rows of one device no expert is named more than 48 times, and in every draw some expert is named exactly 48 times by the rows of some device.
All inputs are finite; a program needn't handle non-finite values.
Results may differ from a plain program's by a relative error of at most 0.015.
The roundings to bfloat16 on the way count: a program that leaves them out, or rounds other values in their place, can miss the bound.
Values may be sent and summed in bfloat16 or wider, within the bound.
A program may use at most 128 MiB of HBM per device.

v0:
```python
import functools

import jax
import jax.numpy as jnp
from jax import lax
from jax.experimental import pallas as pl
from jax.experimental.pallas import tpu as pltpu
from jax.sharding import PartitionSpec as P

GRID_W = 64


rope_base = 10000.0
norm_eps = 1e-06


def head_norm(vectors, gain):
    return (
        vectors * lax.rsqrt(jnp.mean(vectors * vectors, axis=-1, keepdims=True) + norm_eps) * gain
    )


def turn_heads(vectors, positions):
    row_count, head_count, head_size = vectors.shape
    half_size = head_size // 2
    inverse = rope_base ** (-jnp.arange(0, half_size, 2, dtype=jnp.float32) / half_size)
    grid_row = (positions // GRID_W).astype(jnp.float32)
    grid_column = (positions % GRID_W).astype(jnp.float32)
    angles = jnp.concatenate([grid_row[:, None] * inverse, grid_column[:, None] * inverse], axis=-1)
    cosine = jnp.cos(angles)[:, None, :]
    sine = jnp.sin(angles)[:, None, :]
    paired = vectors.reshape(row_count, head_count, half_size, 2)
    first = paired[..., 0]
    second = paired[..., 1]
    turned = jnp.stack([first * cosine - second * sine, first * sine + second * cosine], axis=-1)
    return turned.reshape(vectors.shape)


def slot_ids(route_rows, expert_count, capacity):
    row_count, top_count = route_rows.shape
    flat_routes = route_rows.reshape(-1)
    pair_count = row_count * top_count
    onehot = flat_routes[:, None] == jnp.arange(expert_count, dtype=jnp.int32)[None, :]
    order = jnp.arange(pair_count, dtype=jnp.int32)
    before = (order[None, :] < order[:, None]).astype(jnp.bfloat16)
    earlier = jnp.dot(before, onehot.astype(jnp.bfloat16), preferred_element_type=jnp.float32)
    within = jnp.sum(jnp.where(onehot, earlier, 0.0), axis=1).astype(jnp.int32)
    return (flat_routes * capacity + within).reshape(row_count, top_count)


MESH = pl.DeviceIdType.MESH


def greet(ep_count, tp_count, e, t):
    barrier = pltpu.get_barrier_semaphore()
    peers = 0
    for d in range(1, ep_count):
        pl.semaphore_signal(
            barrier, inc=1, device_id={"ep": lax.rem(e + d, ep_count)}, device_id_type=MESH
        )
        peers += 1
    pair = t // 2
    core = lax.rem(t, 2)
    for k in range(1, tp_count // 2):
        pl.semaphore_signal(
            barrier,
            inc=1,
            device_id={"tp": lax.rem(pair + k, tp_count // 2) * 2 + core},
            device_id_type=MESH,
        )
        peers += 1
    pl.semaphore_signal(
        barrier, inc=1, device_id={"tp": pair * 2 + 1 - core}, device_id_type=MESH
    )
    peers += 1
    pl.semaphore_wait(barrier, peers)


def remote(src, dst, send, recv, device):
    return pltpu.make_async_remote_copy(
        src_ref=src,
        dst_ref=dst,
        send_sem=send,
        recv_sem=recv,
        device_id=device,
        device_id_type=MESH,
    )


def whole_kernel(
    ep_count,
    tp_count,
    blocks,
    normed,
    kv,
    query,
    picking,
    out_weight_hbm,
    gate_hbm,
    up_hbm,
    down_hbm,
    shared_gate_hbm,
    shared_up_hbm,
    shared_down_hbm,
    returned,
    shared_sum,
    mixed_sum,
    arrived,
    normed_all,
    kv_all,
    picking_all,
    out_weight,
    gate,
    up,
    down,
    shared_gate,
    shared_up,
    shared_down,
    heads_scr,
    routed,
    shared,
    mixed,
    routed_pair,
    routed_out,
    routed_in,
    routed_done,
    shared_pair,
    shared_out,
    shared_in,
    mixed_pair,
    mixed_out,
    mixed_in,
    local_sem,
    kv_send,
    kv_recv,
    z_send,
    z_recv,
    x_send,
    x_recv,
    d_send,
    d_recv,
    back_d_send,
    back_d_recv,
    back_x_send,
    back_x_recv,
    back_z_send,
    back_z_recv,
):
    e = lax.axis_index("ep")
    t = lax.axis_index("tp")
    half = tp_count // 2
    pair = t // 2
    core = lax.rem(t, 2)
    sibling = {"tp": pair * 2 + 1 - core}
    f32 = jnp.float32
    bf16 = jnp.bfloat16
    loads = [
        pltpu.make_async_copy(source, target, local_sem.at[3 + n])
        for n, (source, target) in enumerate(
            (
                (out_weight_hbm, out_weight),
                (gate_hbm, gate),
                (up_hbm, up),
                (down_hbm, down),
                (shared_gate_hbm, shared_gate),
                (shared_up_hbm, shared_up),
                (shared_down_hbm, shared_down),
            )
        )
    ]
    for copy in loads:
        copy.start()
    greet(ep_count, tp_count, e, t)

    sends = []

    def send(src, dst, send_sem, recv_sem, device):
        copy = remote(src, dst, send_sem, recv_sem, device)
        copy.start()
        sends.append(copy)

    def landed(spot, recv_sem):
        remote(spot, spot, kv_send.at[0], recv_sem, sibling).wait_recv()

    def source_of(d):
        return lax.rem(e - d + ep_count, ep_count)

    def place(d, row):
        if d == ep_count:
            return normed_all.at[row]
        if d == ep_count + 1:
            return picking_all.at[row]
        return arrived.at[:, row, source_of(d)]

    for d in range(1, ep_count):
        there = lax.rem(e + d, ep_count)
        send(kv, kv_all.at[e], kv_send.at[d], kv_recv.at[e], {"ep": there})
    for d in range(1, ep_count):
        there = lax.rem(e + d, ep_count)
        send(blocks.at[there], arrived.at[:, t, e], z_send.at[d], z_recv.at[e], {"ep": there})

    def spread(src, d):
        for k in range(1, half):
            other = lax.rem(pair + k, half)
            send(
                src,
                place(d, t),
                x_send.at[k, d],
                x_recv.at[pair, d],
                {"tp": other * 2 + core},
            )
        send(src, place(d, t), d_send.at[0, d], d_recv.at[pair, d], sibling)

    def pass_on(d):
        for k in range(1, half):
            other = lax.rem(pair + k, half)
            spot = place(d, other * 2 + core)
            landed(spot, x_recv.at[other, d])
            send(spot, spot, d_send.at[k, d], d_recv.at[other, d], sibling)

    def come(d):
        spot = arrived.at[:, t, source_of(d)]
        landed(spot, z_recv.at[source_of(d)])
        spread(spot, d)

    def all_here(d):
        for other in range(half):
            landed(place(d, other * 2 + 1 - core), d_recv.at[other, d])

    spread(picking, ep_count + 1)
    spread(normed, ep_count)
    own = [
        pltpu.make_async_copy(picking, picking_all.at[t], local_sem.at[0]),
        pltpu.make_async_copy(normed, normed_all.at[t], local_sem.at[1]),
        pltpu.make_async_copy(kv, kv_all.at[e], local_sem.at[2]),
    ]
    for copy in own:
        copy.start()

    query_rows, wide = query.shape[1], query.shape[2]
    model_width = normed.shape[1]
    tile = min(512, model_width)

    def attend(h):
        def step(b, carried):
            top_now, total_now, acc_now = carried
            block = kv_all[b]
            scores = lax.dot_general(
                query[h], block, (((1,), (1,)), ((), ())), preferred_element_type=f32
            )
            top_new = jnp.maximum(top_now, jnp.max(scores, axis=-1, keepdims=True))
            shrink = jnp.exp(top_now - top_new)
            exps = jnp.exp(scores - top_new)
            total_new = total_now * shrink + jnp.sum(exps, axis=-1, keepdims=True)
            acc_new = acc_now * shrink + jnp.dot(
                exps.astype(bf16), block, preferred_element_type=f32
            )
            return (top_new, total_new, acc_new)

        start = (
            jnp.full((query_rows, 1), -1e30, f32),
            jnp.zeros((query_rows, 1), f32),
            jnp.zeros((query_rows, wide), f32),
        )
        top, total, acc = lax.fori_loop(0, ep_count, step, start)
        return acc / total

    def attend_two(n):
        low = pltpu.roll(attend(2 * n), wide // 2, 1)
        high = attend(2 * n + 1)
        lane = lax.broadcasted_iota(jnp.int32, low.shape, 1)
        heads_scr[:, n * wide : (n + 1) * wide] = jnp.where(lane < wide // 2, low, high).astype(
            bf16
        )

    def project():
        def step(n, ignored):
            columns = pl.ds(pl.multiple_of(n * tile, tile), tile)
            part = jnp.dot(heads_scr[...], out_weight[:, columns], preferred_element_type=f32)
            mixed[:, :, columns] = part.astype(bf16).reshape(
                tp_count, query_rows // tp_count, tile
            )
            return ignored

        lax.fori_loop(0, model_width // tile, step, 0)

    local_count, capacity = arrived.shape[0], arrived.shape[3]

    def share():
        def step(row, ignored):
            rows = normed_all[row]
            gate_part = jnp.dot(rows, shared_gate[...], preferred_element_type=f32)
            up_part = jnp.dot(rows, shared_up[...], preferred_element_type=f32)
            hidden = (gate_part / (1.0 + jnp.exp(-gate_part)) * up_part).astype(bf16)
            weight = picking_all[row, 1]
            weight_high = weight.astype(bf16)
            weight_low = (weight - weight_high.astype(f32)).astype(bf16)

            def columns_step(m, inner):
                columns = pl.ds(pl.multiple_of(m * tile, tile), tile)
                results = routed[:, row, e, :, columns]
                if capacity % 16:
                    results = results.astype(f32)
                results = results.reshape(local_count * capacity, tile).astype(bf16)
                part = jnp.dot(hidden, shared_down[:, columns], preferred_element_type=f32)
                part = part + jnp.dot(weight_high, results, preferred_element_type=f32)
                part = part + jnp.dot(weight_low, results, preferred_element_type=f32)
                shared[row, :, columns] = part.astype(bf16)
                return inner

            lax.fori_loop(0, model_width // tile, columns_step, 0)
            return ignored

        lax.fori_loop(0, tp_count, step, 0)

    def pick_own():
        def step(row, ignored):
            chosen = picking_all[row, 0].astype(bf16)

            def columns_step(m, inner):
                columns = pl.ds(pl.multiple_of(m * tile, tile), tile)
                part = lax.dot_general(
                    chosen,
                    normed_all[row, :, columns],
                    (((0,), (0,)), ((), ())),
                    preferred_element_type=f32,
                )
                arrived[:, row, e, :, columns] = part.reshape(local_count, capacity, tile).astype(
                    bf16
                )
                return inner

            lax.fori_loop(0, model_width // tile, columns_step, 0)
            return ignored

        lax.fori_loop(0, tp_count, step, 0)

    def experts(d):
        source = source_of(d)

        def step(n, ignored):
            rows = arrived[n, :, source]
            if capacity % 16:
                rows = rows.astype(f32)
            rows = rows.reshape(tp_count * capacity, model_width).astype(bf16)
            gate_part = jnp.dot(rows, gate[n], preferred_element_type=f32)
            up_part = jnp.dot(rows, up[n], preferred_element_type=f32)
            hidden = (gate_part / (1.0 + jnp.exp(-gate_part)) * up_part).astype(bf16)

            def columns_step(m, inner):
                columns = pl.ds(pl.multiple_of(m * tile, tile), tile)
                part = jnp.dot(hidden, down[n, :, columns], preferred_element_type=f32)
                if capacity % 16:
                    part = part.reshape(tp_count, capacity, tile).astype(bf16)
                else:
                    part = part.astype(bf16).reshape(tp_count, capacity, tile)
                routed[n, :, source, :, columns] = part
                return inner

            lax.fori_loop(0, model_width // tile, columns_step, 0)
            return ignored

        lax.fori_loop(0, local_count, step, 0)

    def item(d):
        if d < ep_count:
            source = source_of(d)
            return (
                lambda row: routed.at[:, row, source],
                lambda k: routed_pair.at[d, k],
                lambda k: routed_out.at[d, k - 1],
                lambda k: routed_in.at[d, k - 1],
            )
        if d == ep_count:
            return (
                lambda row: shared.at[row],
                lambda k: shared_pair.at[k],
                lambda k: shared_out.at[k - 1],
                lambda k: shared_in.at[k - 1],
            )
        return (
            lambda row: mixed.at[row],
            lambda k: mixed_pair.at[k],
            lambda k: mixed_out.at[k - 1],
            lambda k: mixed_in.at[k - 1],
        )

    def to_sibling(d):
        part, paired, out, into = item(d)
        for k in list(range(1, half)) + [0]:
            other = lax.rem(pair + k, half)
            send(
                part(other * 2 + 1 - core),
                paired(k),
                back_d_send.at[d, k],
                back_d_recv.at[d, k],
                sibling,
            )

    def both(d, k):
        part, paired, out, into = item(d)
        spot = paired(k)
        landed(spot, back_d_recv.at[d, k])
        mine = part(lax.rem(pair + k, half) * 2 + core)
        return mine[...].astype(f32) + spot[...].astype(f32)

    crossed = set()

    def across(d):
        if d in crossed:
            return
        crossed.add(d)
        part, paired, out, into = item(d)
        for k in range(1, half):
            other = lax.rem(pair + k, half)
            out(k)[...] = both(d, k).astype(bf16)
            send(
                out(k),
                into(k),
                back_x_send.at[d, k],
                back_x_recv.at[d, k],
                {"tp": other * 2 + core},
            )

    finished = set()

    def finish(d):
        if d in finished:
            return
        finished.add(d)
        part, paired, out, into = item(d)
        total = both(d, 0)
        for k in range(1, half):
            spot = into(k)
            landed(spot, back_x_recv.at[d, k])
            total = total + spot[...].astype(f32)
        if d < ep_count:
            routed_done[d] = total.astype(bf16)
            send(
                routed_done.at[d],
                returned.at[e],
                back_z_send.at[d],
                back_z_recv.at[e],
                {"ep": source_of(d)},
            )
        elif d == ep_count:
            shared_sum[...] = total
        else:
            mixed_sum[...] = total.astype(bf16)

    last = ep_count - 1
    own[2].wait()
    for d in range(1, ep_count):
        landed(kv_all.at[source_of(d)], kv_recv.at[source_of(d)])
    pair_count = query.shape[0] // 2
    for n in range(pair_count):
        attend_two(n)
    pass_on(ep_count + 1)
    pass_on(ep_count)
    loads[0].wait()

    def expert_item(d):
        if d == 0:
            all_here(ep_count + 1)
            all_here(ep_count)
            own[0].wait()
            own[1].wait()
            pick_own()
            for copy in loads[1:]:
                copy.wait()
            experts(0)
            share()
            to_sibling(ep_count)
            returned[e] = jnp.zeros(returned.shape[1:], bf16)
            return
        all_here(d)
        experts(d)
        to_sibling(d)

    for d in range(1, ep_count):
        come(d)
        if d == 1:
            project()
            to_sibling(ep_count + 1)
        else:
            pass_on(d - 1)
            if d == 2:
                across(ep_count + 1)
            expert_item(d - 2)
            if d - 3 >= 1:
                across(d - 3)
    for d in range(1, last - 1):
        across(d)
    expert_item(last - 1)
    pass_on(last)
    across(last - 1)
    expert_item(last)
    for d in range(1, last - 1):
        finish(d)
    across(last)
    across(ep_count)
    across(ep_count + 1)
    for d in list(range(1, ep_count)) + [ep_count, ep_count + 1]:
        finish(d)
    for d in range(1, ep_count):
        landed(returned.at[source_of(d)], back_z_recv.at[source_of(d)])
    for copy in sends:
        copy.wait_send()


def whole(ep_count, tp_count, blocks, normed, kv, query, picking, weights):
    local_count, capacity, width = blocks.shape[1:]
    vmem = pl.BlockSpec(memory_space=pltpu.VMEM)
    anywhere = pl.BlockSpec(memory_space=pl.ANY)
    half = tp_count // 2
    dma = pltpu.SemaphoreType.DMA
    block = (local_count, capacity, width)
    spread_block = (local_count, tp_count, ep_count, capacity, width)
    mixed = (query.shape[1] // tp_count, width)
    count = ep_count + 2

    def room(*shape):
        return pltpu.VMEM(shape, jnp.bfloat16)

    return pl.pallas_call(
        functools.partial(whole_kernel, ep_count, tp_count),
        out_shape=(
            jax.ShapeDtypeStruct((ep_count,) + block, jnp.bfloat16),
            jax.ShapeDtypeStruct(normed.shape, jnp.float32),
            jax.ShapeDtypeStruct(mixed, jnp.bfloat16),
        ),
        in_specs=[vmem] * 5 + [anywhere] * len(weights),
        out_specs=(vmem,) * 3,
        scratch_shapes=[
            room(*spread_block),
            room(tp_count, *normed.shape),
            room(ep_count, *kv.shape),
            pltpu.VMEM((tp_count,) + picking.shape, jnp.float32),
            *[room(*w.shape) for w in weights],
            room(query.shape[1], query.shape[0] // 2 * query.shape[2]),
            room(*spread_block),
            room(tp_count, *normed.shape),
            room(tp_count, *mixed),
            room(ep_count, half, *block),
            room(ep_count, half - 1, *block),
            room(ep_count, half - 1, *block),
            room(ep_count, *block),
            room(half, *normed.shape),
            room(half - 1, *normed.shape),
            room(half - 1, *normed.shape),
            room(half, *mixed),
            room(half - 1, *mixed),
            room(half - 1, *mixed),
            dma((3 + len(weights),)),
            dma((ep_count,)),
            dma((ep_count,)),
            dma((ep_count,)),
            dma((ep_count,)),
            dma((half, ep_count + 2)),
            dma((half, ep_count + 2)),
            dma((half, ep_count + 2)),
            dma((half, ep_count + 2)),
            dma((count, half)),
            dma((count, half)),
            dma((count, half)),
            dma((count, half)),
            dma((ep_count,)),
            dma((ep_count,)),
        ],
        compiler_params=pltpu.CompilerParams(
            collective_id=0, has_side_effects=True, vmem_limit_bytes=67043328
        ),
    )(blocks, normed, kv, query, picking, *weights)


def body(
    queries,
    key_values,
    query_gain,
    key_gain,
    out_weight,
    second_batch,
    norm_gain,
    routes,
    route_weights,
    expert_gate,
    expert_up,
    expert_down,
    shared_gate,
    shared_up,
    shared_down,
):
    query_rows = queries.shape[0]
    head_size = query_gain.shape[0]
    heads_here = queries.shape[1] // head_size
    ep_count = lax.axis_size("ep")
    tp_count = lax.axis_size("tp")
    positions = lax.axis_index("ep") * query_rows + jnp.arange(query_rows, dtype=jnp.int32)
    query_turned = (
        turn_heads(
            head_norm(
                queries.reshape(query_rows, heads_here, head_size).astype(jnp.float32), query_gain
            ),
            positions,
        )
        * head_size ** (-0.5)
    ).astype(jnp.bfloat16)
    key_turned = turn_heads(
        head_norm(key_values[:, None, :head_size].astype(jnp.float32), key_gain), positions
    ).astype(jnp.bfloat16)
    keys_and_values = jnp.concatenate([key_turned[:, 0, :], key_values[:, head_size:]], axis=1)
    tok_count = second_batch.shape[0]
    model_width = second_batch.shape[1]
    top_count = routes.shape[1]
    local_experts = expert_gate.shape[0]
    expert_count = local_experts * ep_count
    capacity = 3 * tok_count * top_count // (2 * expert_count)
    capacity = (capacity + 7) // 8 * 8
    slot_count = expert_count * capacity
    token_float = second_batch.astype(jnp.float32)
    normed = (
        token_float
        * lax.rsqrt(jnp.mean(token_float * token_float, axis=-1, keepdims=True) + norm_eps)
        * norm_gain
    ).astype(jnp.bfloat16)
    own_slots = slot_ids(routes, expert_count, capacity)
    slot_numbers = jnp.arange(slot_count, dtype=jnp.int32)
    picks = [
        (own_slots[:, j][:, None] == slot_numbers[None, :]).astype(jnp.bfloat16)
        for j in range(top_count)
    ]
    outgoing = lax.dot_general(
        sum(picks), normed, (((0,), (0,)), ((), ())), preferred_element_type=jnp.float32
    ).astype(jnp.bfloat16)
    near_count = local_experts * capacity
    near_slots = lax.axis_index("ep") * near_count + jnp.arange(near_count, dtype=jnp.int32)
    near = [own_slots[:, j][:, None] == near_slots[None, :] for j in range(top_count)]
    picking = jnp.stack(
        [
            sum(jnp.where(match, 1.0, 0.0) for match in near),
            sum(
                jnp.where(match, route_weights[:, j : j + 1], 0.0) for j, match in enumerate(near)
            ),
        ]
    )
    query_wide = jnp.pad(
        query_turned.transpose(1, 0, 2), ((0, 0), (0, 0), (0, key_values.shape[1] - head_size))
    )
    returned, shared_sum, mixer_out = whole(
        ep_count,
        tp_count,
        outgoing.reshape(ep_count, local_experts, capacity, model_width),
        normed,
        keys_and_values,
        query_wide,
        picking,
        (
            out_weight,
            expert_gate,
            expert_up,
            expert_down,
            shared_gate,
            shared_up,
            shared_down,
        ),
    )
    returned = returned.reshape(slot_count, model_width)
    combined = shared_sum
    for j in range(top_count):
        combined = combined + route_weights[:, j : j + 1] * jnp.dot(
            picks[j], returned, preferred_element_type=jnp.float32
        )
    return (mixer_out, combined.astype(jnp.bfloat16))


def solution(mesh):
    placed = (
        P(("grp", "ep"), "tp"),
        P(("grp", "ep"), "tp"),
        P(),
        P(),
        P("tp", None),
        P(("grp", "ep", "tp"), None),
        P(),
        P(("grp", "ep", "tp"), None),
        P(("grp", "ep", "tp"), None),
        P("ep", None, "tp"),
        P("ep", None, "tp"),
        P("ep", "tp", None),
        P(None, "tp"),
        P(None, "tp"),
        P("tp", None),
    )
    return jax.shard_map(
        body,
        mesh=mesh,
        in_specs=placed,
        out_specs=(P(("grp", "ep", "tp"), None), P(("grp", "ep", "tp"), None)),
        check_vma=False,
    )
```

profile of v0, /device:TPU:0, one launch (start us, length us, event | category | flops | bytes accessed | tf_op | source)
XLA Modules:
  0.0 135.1 jit_solution(8874780139936047709)
XLA Ops:
  0.7 1.3 fusion.4
  2.0 0.8 slice_bitcast_fusion.1
  2.7 0.8 mul.260
  3.5 0.1 copy.46
  3.6 0.8 copy.37
  4.4 0.1 eq.94
  4.5 0.2 fusion.3
  4.7 0.1 convert_element_type.73
  4.9 0.7 multiply_add_fusion.1
  5.7 0.2 fusion.23
  5.9 0.1 fusion.20
  6.1 0.7 pad_maximum_fusion.picking
  6.7 0.2 copy.44
  7.0 0.2 reshape.618
  7.2 0.1 fusion.8
  7.4 0.2 copy.47
  7.6 0.3 copy.48
  7.9 0.8 pad.4.query
  8.7 0.1 fusion.35
  8.8 0.1 copy.49
  8.9 0.1 fusion.12
  9.1 0.1 fusion.34
  9.2 0.2 subtract_convert_fusion
  9.5 0.1 copy.43
  9.6 0.7 pad_maximum_fusion.1.kv
  10.3 0.2 fusion.6.normed
  10.6 0.8 copy-done.1
  11.4 1.8 %convolution_convert_fusion = bf16[384,2048]{1,0:T(8,128)(2,1)} fusion(bf16[128,2048]{1,0:T(8,128)(2,1)S(1)} %fusion.6.normed, s32[128]{0:T(128)S(1)} %get-tuple-element.27, s32[128]{0:T(128)S(1)} %get-tuple-element.26), kind=kOutput, calls=%fused_computation | convolution fusion | flops 202506240 | bytes 2098176 | tf_op jit(solution)/shard_map/dot_general | solution.py:632
  13.2 117.5 %shard_map.158 = (bf16[4,2,48,2048]{3,2,1,0:T(8,128)(2,1)}, f32[128,2048]{1,0:T(8,128)}, bf16[96,2048]{1,0:T(8,128)(2,1)}) custom-call(bf16[4,2,48,2048]{3,2,1,0:T(8,128)(2,1)} %bitcast.29, bf16[128,2048]{1,0:T(8,128)(2,1)} %copy-done.1, bf16[384,128]{1,0:T(8,128)(2,1)} %pad_maximum_fusion.1.kv, bf16[4,384,128]{2,1,0:T(8,128)(2,1)} %pad.4.query, ...), custom_call_target="tpu_custom_call" | custom-call | tf_op jit(solution)/shard_map/pallas_call | solution.py:525
  130.7 2.3 %fusion.1 = f32[128,2048]{1,0:T(8,128)S(1)} fusion(f32[128,2048]{1,0:T(8,128)} %get-tuple-element.6, bf16[384,2048]{1,0:T(8,128)(2,1)} %bitcast.27, f32[128]{0:T(128)} %copy-done.12, s32[128]{0:T(128)} %copy-done.9), kind=kOutput, calls=%fused_computation.4 | convolution fusion | flops 201900032 | bytes 3671040 | tf_op jit(solution)/shard_map/dot_general | solution.py:670
  133.1 1.3 fusion.2
  134.4 0.7 copy.60
  (45 shorter events, 0.6 us)
Async XLA Ops:
  0.6 6.1 %copy-start.5 = (bf16[384,256]{1,0:T(8,128)(2,1)S(1)}, bf16[384,256]{1,0:T(8,128)(2,1)}, u32[]{:S(2)}) copy-start(bf16[384,256]{1,0:T(8,128)(2,1)} %param.15) | copy-start | bytes 589828
  2.7 3.3 %copy-start.10 = (f32[128]{0:T(128)}, f32[128]{0:T(128)S(1)}, u32[]{:S(2)}) copy-start(f32[128]{0:T(128)S(1)} %get-tuple-element.25) | copy-start | bytes 1540
  2.7 3.3 %copy-start.12 = (f32[128]{0:T(128)}, f32[128]{0:T(128)S(1)}, u32[]{:S(2)}) copy-start(f32[128]{0:T(128)S(1)} %get-tuple-element.24) | copy-start | bytes 1540
  5.6 4.9 %copy-start.7 = (s32[128]{0:T(128)}, s32[128]{0:T(128)S(1)}, u32[]{:S(2)}) copy-start(s32[128]{0:T(128)S(1)} %get-tuple-element.27) | copy-start | bytes 1540
  5.6 4.9 %copy-start.9 = (s32[128]{0:T(128)}, s32[128]{0:T(128)S(1)}, u32[]{:S(2)}) copy-start(s32[128]{0:T(128)S(1)} %get-tuple-element.26) | copy-start | bytes 1540
  7.3 1.4 %copy-start.4 = (bf16[384,128]{1,0:T(8,128)(2,1)S(1)}, bf16[384,128]{1,0:T(8,128)(2,1)}, u32[]{:S(2)}) copy-start(bf16[384,128]{1,0:T(8,128)(2,1)} %param.16) | copy-start | bytes 294916
  7.3 1.6 %copy-start.13 = (f32[64]{0:T(128)S(1)}, f32[64]{0:T(128)}, u32[]{:S(2)}) copy-start(f32[64]{0:T(128)} %param.18) | copy-start | bytes 772
  7.8 2.5 %copy-start.2 = (bf16[128,2048]{1,0:T(8,128)(2,1)S(1)}, bf16[128,2048]{1,0:T(8,128)(2,1)}, u32[]{:S(2)}) copy-start(bf16[128,2048]{1,0:T(8,128)(2,1)} %param.20) | copy-start | bytes 1572868
  7.9 2.5 %copy-start.6 = (f32[2048]{0:T(1024)S(1)}, f32[2048]{0:T(1024)}, u32[]{:S(2)}) copy-start(f32[2048]{0:T(1024)} %param.21) | copy-start | bytes 24580
  10.6 0.8 copy-start.1
  130.7 2.3 %copy-start = (bf16[4,2,48,2048]{3,2,1,0:T(8,128)(2,1)S(1)}, bf16[4,2,48,2048]{3,2,1,0:T(8,128)(2,1)}, u32[]{:S(2)}) copy-start(bf16[4,2,48,2048]{3,2,1,0:T(8,128)(2,1)} %get-tuple-element.7) | copy-start | bytes 4718596
  130.7 2.3 %copy-start.8 = (s32[128]{0:T(128)S(1)}, s32[128]{0:T(128)}, u32[]{:S(2)}) copy-start(s32[128]{0:T(128)} %copy-done.7) | copy-start | bytes 1540
  130.7 2.3 %copy-start.11 = (f32[128]{0:T(128)S(1)}, f32[128]{0:T(128)}, u32[]{:S(2)}) copy-start(f32[128]{0:T(128)} %copy-done.10) | copy-start | bytes 1540
  133.1 1.3 copy-start.3
where the time goes:
time: 135 us
  Pallas kernels  118 us (87%)
  local copies, waits for them, and re-layouts  6.45 us (5%)
  matrix products  5.61 us (4%)
  other arithmetic  4.58 us (3%)
    pallas_call x1, Pallas kernels, whole(): pl.pallas_call(functools.partial(whole_kernel, ep_count, tp_count), out_s...  118 us
    dot_general x2, matrix products, body(): jnp.dot(picks[j], returned, preferred_element_type=jnp.float32)  3.59 us

commit v1 on v0

v1 whole, which is shorter than its diff:
```python
import functools
import math

import jax
import jax.numpy as jnp
from jax import lax
from jax.experimental import pallas as pl
from jax.experimental.pallas import tpu as pltpu
from jax.sharding import PartitionSpec as P

GRID_W = 64


rope_base = 10000.0
norm_eps = 1e-06

MESH = pl.DeviceIdType.MESH


def greet(ep_count, tp_count, e, t):
    barrier = pltpu.get_barrier_semaphore()
    peers = 0
    for d in range(1, ep_count):
        pl.semaphore_signal(
            barrier, inc=1, device_id={"ep": lax.rem(e + d, ep_count)}, device_id_type=MESH
        )
        peers += 1
    pair = t // 2
    core = lax.rem(t, 2)
    for k in range(1, tp_count // 2):
        pl.semaphore_signal(
            barrier,
            inc=1,
            device_id={"tp": lax.rem(pair + k, tp_count // 2) * 2 + core},
            device_id_type=MESH,
        )
        peers += 1
    pl.semaphore_signal(
        barrier, inc=1, device_id={"tp": pair * 2 + 1 - core}, device_id_type=MESH
    )
    peers += 1
    return lambda: pl.semaphore_wait(barrier, peers)


def remote(src, dst, send, recv, device):
    return pltpu.make_async_remote_copy(
        src_ref=src,
        dst_ref=dst,
        send_sem=send,
        recv_sem=recv,
        device_id=device,
        device_id_type=MESH,
    )


def whole_kernel(
    ep_count,
    tp_count,
    direct,
    queries_hbm,
    kv_hbm,
    query_gain_hbm,
    key_gain_hbm,
    batch_hbm,
    norm_gain_hbm,
    routes_hbm,
    route_weights_hbm,
    out_weight_hbm,
    gate_hbm,
    up_hbm,
    down_hbm,
    shared_gate_hbm,
    shared_up_hbm,
    shared_down_hbm,
    channel_out,
    mixed_sum,
    queries,
    kv_in,
    head_gains,
    batch,
    norm_gain,
    routes,
    route_weights,
    tables,
    query,
    tokens,
    arrived,
    normed_all,
    kv_all,
    meta_ep,
    meta_tp,
    out_weight,
    gate,
    up,
    down,
    shared_both,
    shared_down,
    heads_scr,
    routed,
    shared,
    mixed,
    combined,
    returned,
    routed_pair,
    routed_out,
    routed_in,
    routed_done,
    shared_pair,
    shared_out,
    shared_in,
    mixed_pair,
    mixed_out,
    mixed_in,
    local_sem,
    kv_send,
    kv_recv,
    meta_send,
    meta_recv,
    z_send,
    z_recv,
    x_send,
    x_recv,
    d_send,
    d_recv,
    back_d_send,
    back_d_recv,
    back_x_send,
    back_x_recv,
    back_z_send,
    back_z_recv,
):
    e = lax.axis_index("ep")
    t = lax.axis_index("tp")
    half = tp_count // 2
    pair = t // 2
    core = lax.rem(t, 2)
    sibling = {"tp": pair * 2 + 1 - core}
    f32 = jnp.float32
    bf16 = jnp.bfloat16
    head_size = query_gain_hbm.shape[1]
    shared_width = shared_down.shape[0]
    loads = [
        pltpu.make_async_copy(source, target, local_sem.at[n])
        for n, (source, target) in enumerate(
            (
                (batch_hbm, batch),
                (norm_gain_hbm, norm_gain),
                (routes_hbm, routes),
                (route_weights_hbm, route_weights),
                (kv_hbm, kv_in),
                (query_gain_hbm, head_gains.at[0]),
                (key_gain_hbm, head_gains.at[1]),
                (queries_hbm, queries),
                (shared_gate_hbm, shared_both.at[:, :shared_width]),
                (shared_up_hbm, shared_both.at[:, shared_width:]),
                (gate_hbm, gate),
                (up_hbm, up),
                (down_hbm, down),
                (shared_down_hbm, shared_down),
                (out_weight_hbm, out_weight),
            )
        )
    ]
    for copy in loads:
        copy.start()
    greeted = greet(ep_count, tp_count, e, t)

    sends = []

    def send(src, dst, send_sem, recv_sem, device):
        copy = remote(src, dst, send_sem, recv_sem, device)
        copy.start()
        sends.append((None, copy.wait_send))

    def send_if(wanted, make):
        @pl.when(wanted)
        def _():
            make().start()

        sends.append((wanted, lambda: make().wait_send()))

    def landed(spot, recv_sem):
        remote(spot, spot, kv_send.at[0], recv_sem, sibling).wait_recv()

    near_side = jnp.minimum(e, ep_count - 1 - e)
    far_way = jnp.where(e < ep_count - 1 - e, 1, -1)

    def source_of(d):
        if d == 0:
            return e
        way = -1 if d % 2 else 1
        return jnp.where(
            d <= 2 * near_side, e + way * ((d + 1) // 2), e + far_way * (d - near_side)
        )

    tok_count, model_width = batch.shape
    local_count, capacity = arrived.shape[0], arrived.shape[3]
    near_count = local_count * capacity
    tile = min(512, model_width)

    def tiles(step):
        def run(m, ignored):
            step(pl.ds(pl.multiple_of(m * tile, tile), tile))
            return ignored

        lax.fori_loop(0, model_width // tile, run, 0)

    def picks_of(meta, rank, ranks=1):
        rows = ranks * near_count
        numbers = lax.broadcasted_iota(jnp.int32, (rows, tok_count), 0)
        expert = (numbers // capacity + rank * local_count).astype(f32)
        place = lax.rem(numbers, capacity).astype(f32)
        earlier = lax.broadcasted_iota(jnp.int32, (tok_count, tok_count), 0)
        later = lax.broadcasted_iota(jnp.int32, (tok_count, tok_count), 1)
        before = jnp.where(earlier < later, 1.0, 0.0).astype(bf16)
        named = [meta[j : j + 1, :] == expert for j in range(2)]
        any_named = sum(jnp.where(match, 1.0, 0.0) for match in named)
        count = jnp.dot(any_named.astype(bf16), before, preferred_element_type=f32)
        picked = jnp.where(count == place, any_named, 0.0)
        weight = sum(jnp.where(match, meta[2 + j : 3 + j, :], 0.0) for j, match in enumerate(named))
        return picked, picked * weight

    def split(value):
        high = value.astype(bf16)
        return high, (value - high.astype(f32)).astype(bf16)

    def place(d, row):
        if d == ep_count:
            return normed_all.at[row]
        if d == ep_count + 1:
            return meta_tp.at[row]
        return arrived.at[:, row, source_of(d)]

    def spread(src, d):
        for k in range(1, half):
            other = lax.rem(pair + k, half)
            send(
                src,
                place(d, t),
                x_send.at[k, d],
                x_recv.at[pair, d],
                {"tp": other * 2 + core},
            )
        send(src, place(d, t), d_send.at[0, d], d_recv.at[pair, d], sibling)

    def pass_on(d):
        for k in range(1, half):
            other = lax.rem(pair + k, half)
            spot = place(d, other * 2 + core)
            landed(spot, x_recv.at[other, d])
            send(spot, spot, d_send.at[k, d], d_recv.at[other, d], sibling)

    def all_here(d):
        for other in range(half):
            landed(place(d, other * 2 + 1 - core), d_recv.at[other, d])

    loads[0].wait()
    loads[1].wait()
    norm_rows = math.gcd(tok_count, 16)

    def norm_step(n, ignored):
        rows = pl.ds(pl.multiple_of(n * norm_rows, norm_rows), norm_rows)
        value = batch[rows, :].astype(f32)
        scale = lax.rsqrt(jnp.mean(value * value, axis=-1, keepdims=True) + norm_eps)
        normed_all[t, rows, :] = (value * scale * norm_gain[...]).astype(bf16)
        return ignored

    lax.fori_loop(0, tok_count // norm_rows, norm_step, 0)
    loads[2].wait()
    loads[3].wait()
    meta_tp[t, 0:2, :] = routes[...].astype(f32)
    meta_tp[t, 2:4, :] = route_weights[...]
    greeted()
    spread(normed_all.at[t], ep_count)
    if not direct:
        send_if(
            e < ep_count - 1,
            lambda: remote(
                normed_all.at[t], tokens.at[e], z_send.at[e], z_recv.at[e], {"ep": e + 1}
            ),
        )
        send_if(
            e > 0,
            lambda: remote(
                normed_all.at[t], tokens.at[e], z_send.at[ep_count], z_recv.at[e], {"ep": e - 1}
            ),
        )
    spread(meta_tp.at[t], ep_count + 1)
    if direct:
        picked, ignored_weight = picks_of(meta_tp[t], 0, ep_count)
        picked = picked.astype(bf16)

        def block_step(columns):
            part = jnp.dot(picked, normed_all[t, :, columns], preferred_element_type=f32)
            tokens[:, :, :, columns] = part.reshape(
                ep_count, local_count, capacity, tile
            ).astype(bf16)

        tiles(block_step)
        for d in range(1, ep_count):
            there = lax.rem(e + d, ep_count)
            send(
                tokens.at[there], arrived.at[:, t, e], z_send.at[d], z_recv.at[e], {"ep": there}
            )
    else:
        for d in range(1, ep_count):
            there = lax.rem(e + d, ep_count)
            send(meta_tp.at[t], meta_ep.at[e], meta_send.at[d], meta_recv.at[e], {"ep": there})

    query_rows, wide = query.shape[1], query.shape[2]
    groups = query_rows // GRID_W
    lane = lax.broadcasted_iota(jnp.int32, (GRID_W, wide), 1)
    low = lane < head_size

    def turn_tables():
        in_head = lax.rem(lane, head_size)
        step = lax.rem(in_head // 2, head_size // 4).astype(f32)
        inverse = jnp.exp(step * (-4.0 / head_size * math.log(rope_base)))
        number = lax.broadcasted_iota(jnp.int32, (GRID_W, wide), 0)
        sign = jnp.where(lax.rem(lane, 2) == 0, -1.0, 1.0)
        column_angle = number.astype(f32) * inverse
        tables[0] = jnp.cos(column_angle)
        tables[1] = jnp.sin(column_angle) * sign
        short = tables.shape[1] // 4
        row_angle = (number + e * groups).astype(f32)[:short] * inverse[:short]
        tables[2, :short] = jnp.cos(row_angle)
        tables[3, :short] = jnp.sin(row_angle) * sign[:short]

    def turn(value, group):
        by_row = lax.rem(lane, head_size) < head_size // 2
        cosine = jnp.where(by_row, tables[2, pl.ds(group, 1), :], tables[0])
        sine = jnp.where(by_row, tables[3, pl.ds(group, 1), :], tables[1])
        swapped = jnp.where(
            lax.rem(lane, 2) == 0, pltpu.roll(value, wide - 1, 1), pltpu.roll(value, 1, 1)
        )
        return value * cosine + swapped * sine

    def gain_of(n):
        value = head_gains[n]
        return jnp.concatenate([value] * (wide // head_size), axis=1)

    for n in (4, 5, 6):
        loads[n].wait()
    turn_tables()

    def key_step(group, ignored):
        rows = pl.ds(pl.multiple_of(group * GRID_W, GRID_W), GRID_W)
        value = kv_in[rows, :].astype(f32)
        square = jnp.sum(jnp.where(low, value * value, 0.0), axis=-1, keepdims=True)
        scaled = value * lax.rsqrt(square / head_size + norm_eps) * gain_of(1)
        kv_all[e, rows, :] = jnp.where(low, turn(scaled, group), value).astype(bf16)
        return ignored

    lax.fori_loop(0, groups, key_step, 0)
    for d in range(1, ep_count):
        there = lax.rem(e + d, ep_count)
        send(kv_all.at[e], kv_all.at[e], kv_send.at[d], kv_recv.at[e], {"ep": there})
    loads[7].wait()

    def query_step(group, ignored):
        rows = pl.ds(pl.multiple_of(group * GRID_W, GRID_W), GRID_W)
        for n in range(query.shape[0] // 2):
            value = queries[rows, n * wide : (n + 1) * wide].astype(f32)
            square = value * value
            sums = [
                jnp.sum(jnp.where(side, square, 0.0), axis=-1, keepdims=True)
                for side in (low, jnp.logical_not(low))
            ]
            scales = [lax.rsqrt(total / head_size + norm_eps) for total in sums]
            scaled = value * jnp.where(low, scales[0], scales[1]) * gain_of(0)
            turned = turn(scaled, group) * head_size ** (-0.5)
            query[2 * n, rows, :] = jnp.where(low, turned, 0.0).astype(bf16)
            query[2 * n + 1, rows, :] = jnp.where(
                low, pltpu.roll(turned, wide // 2, 1), 0.0
            ).astype(bf16)
        return ignored

    lax.fori_loop(0, groups, query_step, 0)

    def come(d):
        source = source_of(d)
        spot = arrived.at[:, t, source]
        if direct:
            landed(spot, z_recv.at[source])
        else:
            landed(tokens.at[source], z_recv.at[source])
            above = source > e
            send_if(
                jnp.logical_or(
                    jnp.logical_and(above, e > 0),
                    jnp.logical_and(jnp.logical_not(above), e < ep_count - 1),
                ),
                lambda: remote(
                    tokens.at[source],
                    tokens.at[source],
                    z_send.at[source],
                    z_recv.at[source],
                    {"ep": jnp.where(source > e, e - 1, e + 1)},
                ),
            )
            landed(meta_ep.at[source], meta_recv.at[source])
            picked, ignored_weight = picks_of(meta_ep[source], e)
            picked = picked.astype(bf16)

            def pick_step(columns):
                part = jnp.dot(picked, tokens[source, :, columns], preferred_element_type=f32)
                arrived[:, t, source, :, columns] = part.reshape(
                    local_count, capacity, tile
                ).astype(bf16)

            tiles(pick_step)
        spread(spot, d)

    def attend(h):
        def step(b, carried):
            top_now, total_now, acc_now = carried
            block = kv_all[b]
            scores = lax.dot_general(
                query[h], block, (((1,), (1,)), ((), ())), preferred_element_type=f32
            )
            top_new = jnp.maximum(top_now, jnp.max(scores, axis=-1, keepdims=True))
            shrink = jnp.exp(top_now - top_new)
            exps = jnp.exp(scores - top_new)
            total_new = total_now * shrink + jnp.sum(exps, axis=-1, keepdims=True)
            acc_new = acc_now * shrink + jnp.dot(
                exps.astype(bf16), block, preferred_element_type=f32
            )
            return (top_new, total_new, acc_new)

        start = (
            jnp.full((query_rows, 1), -1e30, f32),
            jnp.zeros((query_rows, 1), f32),
            jnp.zeros((query_rows, wide), f32),
        )
        top, total, acc = lax.fori_loop(0, ep_count, step, start)
        return acc / total

    def attend_two(n):
        low = pltpu.roll(attend(2 * n), wide // 2, 1)
        high = attend(2 * n + 1)
        lane = lax.broadcasted_iota(jnp.int32, low.shape, 1)
        heads_scr[:, n * wide : (n + 1) * wide] = jnp.where(lane < wide // 2, low, high).astype(
            bf16
        )

    def project():
        def step(n, ignored):
            columns = pl.ds(pl.multiple_of(n * tile, tile), tile)
            part = jnp.dot(heads_scr[...], out_weight[:, columns], preferred_element_type=f32)
            mixed[:, :, columns] = part.astype(bf16).reshape(
                tp_count, query_rows // tp_count, tile
            )
            return ignored

        lax.fori_loop(0, model_width // tile, step, 0)

    def share():
        def step(row, ignored):
            both_parts = jnp.dot(normed_all[row], shared_both[...], preferred_element_type=f32)
            gate_part = both_parts[:, :shared_width]
            up_part = both_parts[:, shared_width:]
            hidden = (gate_part / (1.0 + jnp.exp(-gate_part)) * up_part).astype(bf16)
            ignored_pick, weight = picks_of(meta_tp[row], e)
            weights = split(weight)

            def columns_step(columns):
                results = routed[:, row, e, :, columns]
                if capacity % 16:
                    results = results.astype(f32)
                results = results.reshape(near_count, tile).astype(bf16)
                part = jnp.dot(hidden, shared_down[:, columns], preferred_element_type=f32)
                for one in weights:
                    part = part + lax.dot_general(
                        one, results, (((0,), (0,)), ((), ())), preferred_element_type=f32
                    )
                shared[row, :, columns] = part.astype(bf16)

            tiles(columns_step)
            return ignored

        lax.fori_loop(0, tp_count, step, 0)

    def pick_own():
        def step(row, ignored):
            picked, ignored_weight = picks_of(meta_tp[row], e)
            picked = picked.astype(bf16)

            def columns_step(columns):
                part = jnp.dot(picked, normed_all[row, :, columns], preferred_element_type=f32)
                arrived[:, row, e, :, columns] = part.reshape(
                    local_count, capacity, tile
                ).astype(bf16)

            tiles(columns_step)
            return ignored

        lax.fori_loop(0, tp_count, step, 0)

    def experts(d):
        source = source_of(d)

        def step(n, ignored):
            rows = arrived[n, :, source]
            if capacity % 16:
                rows = rows.astype(f32)
            rows = rows.reshape(tp_count * capacity, model_width).astype(bf16)
            gate_part = jnp.dot(rows, gate[n], preferred_element_type=f32)
            up_part = jnp.dot(rows, up[n], preferred_element_type=f32)
            hidden = (gate_part / (1.0 + jnp.exp(-gate_part)) * up_part).astype(bf16)

            def columns_step(m, inner):
                columns = pl.ds(pl.multiple_of(m * tile, tile), tile)
                part = jnp.dot(hidden, down[n, :, columns], preferred_element_type=f32)
                if capacity % 16:
                    part = part.reshape(tp_count, capacity, tile).astype(bf16)
                else:
                    part = part.astype(bf16).reshape(tp_count, capacity, tile)
                routed[n, :, source, :, columns] = part
                return inner

            lax.fori_loop(0, model_width // tile, columns_step, 0)
            return ignored

        lax.fori_loop(0, local_count, step, 0)

    def item(d):
        if d < ep_count:
            source = source_of(d)
            return (
                lambda row: routed.at[:, row, source],
                lambda k: routed_pair.at[d, k],
                lambda k: routed_out.at[d, k - 1],
                lambda k: routed_in.at[d, k - 1],
            )
        if d == ep_count:
            return (
                lambda row: shared.at[row],
                lambda k: shared_pair.at[k],
                lambda k: shared_out.at[k - 1],
                lambda k: shared_in.at[k - 1],
            )
        return (
            lambda row: mixed.at[row],
            lambda k: mixed_pair.at[k],
            lambda k: mixed_out.at[k - 1],
            lambda k: mixed_in.at[k - 1],
        )

    def to_sibling(d):
        part, paired, out, into = item(d)
        for k in list(range(1, half)) + [0]:
            other = lax.rem(pair + k, half)
            send(
                part(other * 2 + 1 - core),
                paired(k),
                back_d_send.at[d, k],
                back_d_recv.at[d, k],
                sibling,
            )

    def both(d, k):
        part, paired, out, into = item(d)
        spot = paired(k)
        landed(spot, back_d_recv.at[d, k])
        mine = part(lax.rem(pair + k, half) * 2 + core)
        return mine[...].astype(f32) + spot[...].astype(f32)

    def across(d):
        part, paired, out, into = item(d)
        for k in range(1, half):
            other = lax.rem(pair + k, half)
            out(k)[...] = both(d, k).astype(bf16)
            send(
                out(k),
                into(k),
                back_x_send.at[d, k],
                back_x_recv.at[d, k],
                {"tp": other * 2 + core},
            )

    def finish(d):
        part, paired, out, into = item(d)
        total = both(d, 0)
        for k in range(1, half):
            spot = into(k)
            landed(spot, back_x_recv.at[d, k])
            total = total + spot[...].astype(f32)
        if d < ep_count:
            routed_done[d] = total.astype(bf16)
            send(
                routed_done.at[d],
                returned.at[e],
                back_z_send.at[d],
                back_z_recv.at[e],
                {"ep": source_of(d)},
            )
        elif d == ep_count:
            channel_out[...] = (total + combined[...]).astype(bf16)
        else:
            mixed_sum[...] = total.astype(bf16)

    def combine(d):
        source = source_of(d)
        landed(returned.at[source], back_z_recv.at[source])
        ignored_pick, weight = picks_of(meta_tp[t], source)
        weights = split(weight)

        def columns_step(columns):
            results = returned[source, :, :, columns]
            if capacity % 16:
                results = results.astype(f32)
            results = results.reshape(near_count, tile).astype(bf16)
            part = sum(
                lax.dot_general(
                    one, results, (((0,), (0,)), ((), ())), preferred_element_type=f32
                )
                for one in weights
            )
            combined[:, columns] = part if d == 1 else combined[:, columns] + part

        tiles(columns_step)

    last = ep_count - 1
    pair_count = query.shape[0] // 2

    def expert_item(d):
        all_here(d)
        experts(d)
        to_sibling(d)

    def attention():
        for d in range(1, ep_count):
            landed(kv_all.at[source_of(d)], kv_recv.at[source_of(d)])
        for n in range(pair_count):
            attend_two(n)
        loads[14].wait()
        project()
        to_sibling(ep_count + 1)

    pass_on(ep_count + 1)
    pass_on(ep_count)
    come(1)
    all_here(ep_count + 1)
    all_here(ep_count)
    pick_own()
    for n in range(8, 14):
        loads[n].wait()
    experts(0)
    share()
    to_sibling(ep_count)
    for d in range(2, ep_count):
        come(d)
        pass_on(d - 1)
        expert_item(d - 1)
        across(d - 1)
        if d == 2:
            attention()
        if d > 2:
            finish(d - 2)
    pass_on(last)
    expert_item(last)
    across(last)
    across(ep_count + 1)
    across(ep_count)
    for d in range(max(1, last - 1), ep_count):
        finish(d)
    finish(ep_count + 1)
    for d in range(1, ep_count):
        combine(d)
    finish(ep_count)
    for wanted, wait in sends:
        if wanted is None:
            wait()
        else:
            pl.when(wanted)(wait)


def whole(ep_count, tp_count, small, weights):
    queries, key_values, query_gain, key_gain, batch, norm_gain, routes, route_weights = small
    out_weight, gate, up, down, shared_gate, shared_up, shared_down = weights
    local_count = gate.shape[0]
    tok_count, width = batch.shape
    query_rows, wide = key_values.shape
    head_size = query_gain.shape[1]
    heads_here = queries.shape[1] // head_size
    expert_count = local_count * ep_count
    capacity = 3 * tok_count * routes.shape[0] // (2 * expert_count)
    capacity = (capacity + 7) // 8 * 8
    direct = 2 * local_count * capacity <= tok_count
    anywhere = pl.BlockSpec(memory_space=pl.ANY)
    half = tp_count // 2
    dma = pltpu.SemaphoreType.DMA
    block = (local_count, capacity, width)
    spread_block = (local_count, tp_count, ep_count, capacity, width)
    token_block = (tok_count, width)
    mixed = (query_rows // tp_count, width)
    count = ep_count + 2

    def room(*shape):
        return pltpu.VMEM(shape, jnp.bfloat16)

    def wide_room(*shape):
        return pltpu.VMEM(shape, jnp.float32)

    return pl.pallas_call(
        functools.partial(whole_kernel, ep_count, tp_count, direct),
        out_shape=(
            jax.ShapeDtypeStruct(token_block, jnp.bfloat16),
            jax.ShapeDtypeStruct(mixed, jnp.bfloat16),
        ),
        in_specs=[anywhere] * (len(small) + len(weights)),
        out_specs=(pl.BlockSpec(memory_space=pltpu.VMEM),) * 2,
        scratch_shapes=[
            room(*queries.shape),
            room(*key_values.shape),
            wide_room(2, 1, head_size),
            room(*batch.shape),
            wide_room(*norm_gain.shape),
            pltpu.VMEM(routes.shape, jnp.int32),
            wide_room(*route_weights.shape),
            wide_room(4, GRID_W, wide),
            room(heads_here, query_rows, wide),
            room(*((ep_count,) + (block if direct else token_block))),
            room(*spread_block),
            room(tp_count, *token_block),
            room(ep_count, *key_values.shape),
            wide_room(ep_count, 8, tok_count),
            wide_room(tp_count, 8, tok_count),
            room(*out_weight.shape),
            room(*gate.shape),
            room(*up.shape),
            room(*down.shape),
            room(shared_gate.shape[0], 2 * shared_gate.shape[1]),
            room(*shared_down.shape),
            room(query_rows, heads_here // 2 * wide),
            room(*spread_block),
            room(tp_count, *token_block),
            room(tp_count, *mixed),
            wide_room(*token_block),
            room(ep_count, *block),
            room(ep_count, half, *block),
            room(ep_count, half - 1, *block),
            room(ep_count, half - 1, *block),
            room(ep_count, *block),
            room(half, *token_block),
            room(half - 1, *token_block),
            room(half - 1, *token_block),
            room(half, *mixed),
            room(half - 1, *mixed),
            room(half - 1, *mixed),
            dma((len(small) + len(weights),)),
            dma((ep_count,)),
            dma((ep_count,)),
            dma((ep_count,)),
            dma((ep_count,)),
            dma((ep_count + 1,)),
            dma((ep_count,)),
            dma((half, ep_count + 2)),
            dma((half, ep_count + 2)),
            dma((half, ep_count + 2)),
            dma((half, ep_count + 2)),
            dma((count, half)),
            dma((count, half)),
            dma((count, half)),
            dma((count, half)),
            dma((ep_count,)),
            dma((ep_count,)),
        ],
        compiler_params=pltpu.CompilerParams(
            collective_id=0, has_side_effects=True, vmem_limit_bytes=67043328
        ),
    )(*small, *weights)


def body(
    queries,
    key_values,
    query_gain,
    key_gain,
    out_weight,
    second_batch,
    norm_gain,
    routes,
    route_weights,
    expert_gate,
    expert_up,
    expert_down,
    shared_gate,
    shared_up,
    shared_down,
):
    channel_out, mixer_out = whole(
        lax.axis_size("ep"),
        lax.axis_size("tp"),
        (
            queries,
            key_values,
            query_gain[None, :],
            key_gain[None, :],
            second_batch,
            norm_gain[None, :],
            routes.T,
            route_weights.T,
        ),
        (
            out_weight,
            expert_gate,
            expert_up,
            expert_down,
            shared_gate,
            shared_up,
            shared_down,
        ),
    )
    return (mixer_out, channel_out)


def solution(mesh):
    placed = (
        P(("grp", "ep"), "tp"),
        P(("grp", "ep"), "tp"),
        P(),
        P(),
        P("tp", None),
        P(("grp", "ep", "tp"), None),
        P(),
        P(("grp", "ep", "tp"), None),
        P(("grp", "ep", "tp"), None),
        P("ep", None, "tp"),
        P("ep", None, "tp"),
        P("ep", "tp", None),
        P(None, "tp"),
        P(None, "tp"),
        P("tp", None),
    )
    return jax.shard_map(
        body,
        mesh=mesh,
        in_specs=placed,
        out_specs=(P(("grp", "ep", "tp"), None), P(("grp", "ep", "tp"), None)),
        check_vma=False,
    )
```

time: 135 us -> 117 us (0.87)
  Pallas kernels: 118 us -> 112 us
  matrix products: 5.61 us -> 0 us
  other arithmetic: 4.58 us -> 0 us
  local copies, waits for them, and re-layouts: 6.45 us -> 3.65 us
    dot_general x4 -> x0, matrix products: 5.61 us -> none  [the longest x2 3.59 us: body(): jnp.dot(picks[j], returned, preferred_element_type=jnp.float32)]
    pallas_call x1, Pallas kernels: 118 us -> 112 us  [whole(): pl.pallas_call(functools.partial(whole_kernel, ep_count, tp_count, direct...]
    reduce_sum x3 -> x0, other arithmetic: 1.37 us -> none  [the longest x1 1.28 us: body(): jnp.mean(token_float * token_float, axis=-1, keepdims=True) + norm_eps]
    unnamed x32 -> x2, local copies, waits for them, and re-layouts: 2.65 us -> 3.65 us
where the time goes in v1:
time: 117 us
  Pallas kernels  112 us (96%)
  local copies, waits for them, and re-layouts  3.65 us (3%)
    pallas_call x1, Pallas kernels, whole(): pl.pallas_call(functools.partial(whole_kernel, ep_count, tp_count, direct...  112 us
    unnamed x2, local copies, waits for them, and re-layouts  3.65 us

profile of v1, /device:TPU:0, one launch (start us, length us, event | category | flops | bytes accessed | tf_op | source)
XLA Modules:
  0.0 116.6 jit_solution(10793087350822470587)
XLA Ops:
  0.6 112.4 %shard_map.158 = (bf16[128,2048]{1,0:T(8,128)(2,1)}, bf16[96,2048]{1,0:T(8,128)(2,1)}) custom-call(bf16[384,256]{1,0:T(8,128)(2,1)} %queries_hbm.1, bf16[384,128]{1,0:T(8,128)(2,1)} %kv_hbm.1, f32[1,64]{1,0:T(1,128)} %bitcast.8, f32[1,64]{1,0:T(1,128)} %bitcast.9, bf16[128,2048]{1,0:T(8,128)(2,1)} %batch_hbm.1, f32[1,2048]{1,0:T(1,128)} %bitcast.5, ...), custom_call_target="tpu_custom_call" | custom-call | tf_op jit(solution)/shard_map/pallas_call | solution.py:705
  113.0 1.8 %copy.19 = bf16[96,2048]{1,0:T(8,128)(2,1)} copy(bf16[96,2048]{1,0:T(8,128)(2,1)} %get-tuple-element.8) | data formatting | bytes 786432
  114.8 1.9 %copy.20 = bf16[128,2048]{1,0:T(8,128)(2,1)} copy(bf16[128,2048]{1,0:T(8,128)(2,1)} %get-tuple-element.9) | data formatting | bytes 1048576

commit v2 on v1

--- a/solution.py
+++ b/solution.py
@@ -99,8 +99,13 @@
     routed,
     shared,
     mixed,
+    hidden,
+    weights_here,
     combined,
     returned,
+    onward,
+    lent_out,
+    lent_in,
     routed_pair,
     routed_out,
     routed_in,
@@ -116,6 +121,10 @@
     kv_recv,
     meta_send,
     meta_recv,
+    lent_send,
+    lent_recv,
+    r_send,
+    r_recv,
     z_send,
     z_recv,
     x_send,
@@ -167,10 +176,28 @@
 
     sends = []
 
+    state = {"start": True, "note": True, "when": None}
+
     def send(src, dst, send_sem, recv_sem, device):
         copy = remote(src, dst, send_sem, recv_sem, device)
-        copy.start()
-        sends.append((None, copy.wait_send))
+        if state["start"]:
+            copy.start()
+        if state["note"]:
+            sends.append((state["when"], copy.wait_send))
+
+    def branch(when, *steps):
+        @pl.when(when)
+        def _():
+            state["note"] = False
+            for step in steps:
+                step()
+            state["note"] = True
+
+    def note(when, *steps):
+        state.update(start=False, when=when)
+        for step in steps:
+            step()
+        state.update(start=True, when=None)
 
     def send_if(wanted, make):
         @pl.when(wanted)
@@ -180,7 +207,8 @@
         sends.append((wanted, lambda: make().wait_send()))
 
     def landed(spot, recv_sem):
-        remote(spot, spot, kv_send.at[0], recv_sem, sibling).wait_recv()
+        if state["start"]:
+            remote(spot, spot, kv_send.at[0], recv_sem, sibling).wait_recv()
 
     near_side = jnp.minimum(e, ep_count - 1 - e)
     far_way = jnp.where(e < ep_count - 1 - e, 1, -1)
@@ -188,22 +216,29 @@
     def source_of(d):
         if d == 0:
             return e
-        way = -1 if d % 2 else 1
+        way = far_way if d % 2 else -far_way
         return jnp.where(
             d <= 2 * near_side, e + way * ((d + 1) // 2), e + far_way * (d - near_side)
         )
+
+    def first_of(rank):
+        inner = jnp.where(rank < ep_count - 1 - rank, rank - 1, rank + 1)
+        return jnp.where(rank == 0, 1, jnp.where(rank == ep_count - 1, ep_count - 2, inner))
 
     tok_count, model_width = batch.shape
     local_count, capacity = arrived.shape[0], arrived.shape[3]
     near_count = local_count * capacity
     tile = min(512, model_width)
 
-    def tiles(step):
+    def tiles(step, first=0, stop=model_width):
         def run(m, ignored):
             step(pl.ds(pl.multiple_of(m * tile, tile), tile))
             return ignored
 
-        lax.fori_loop(0, model_width // tile, run, 0)
+        lax.fori_loop(first // tile, stop // tile, run, 0)
+
+    half_width = model_width // 2
+    sides = [(c * half_width, (c + 1) * half_width) for c in range(2)]
 
     def picks_of(meta, rank, ranks=1):
         rows = ranks * near_count
@@ -250,8 +285,9 @@
             landed(spot, x_recv.at[other, d])
             send(spot, spot, d_send.at[k, d], d_recv.at[other, d], sibling)
 
-    def all_here(d):
-        for other in range(half):
+    def all_here(d, kinds=range(half)):
+        for k in kinds:
+            other = lax.rem(pair + k, half)
             landed(place(d, other * 2 + 1 - core), d_recv.at[other, d])
 
     loads[0].wait()
@@ -352,9 +388,6 @@
         return ignored
 
     lax.fori_loop(0, groups, key_step, 0)
-    for d in range(1, ep_count):
-        there = lax.rem(e + d, ep_count)
-        send(kv_all.at[e], kv_all.at[e], kv_send.at[d], kv_recv.at[e], {"ep": there})
     loads[7].wait()
 
     def query_step(group, ignored):
@@ -377,39 +410,108 @@
 
     lax.fori_loop(0, groups, query_step, 0)
 
+    early = near_side > 0
+    late = jnp.logical_not(early)
+
+    def pick_into(source, rank, target, first=0, stop=model_width):
+        picked, ignored_weight = picks_of(meta_ep[source], rank)
+        picked = picked.astype(bf16)
+
+        def pick_step(columns):
+            part = jnp.dot(picked, tokens[source, :, columns], preferred_element_type=f32)
+            target(columns, part.reshape(local_count, capacity, tile).astype(bf16))
+
+        tiles(pick_step, first, stop)
+
+    def relay(d, parts=(0, 1)):
+        if direct:
+            return
+        source = source_of(d)
+        target = jnp.where(source > e, e - 1, e + 1)
+        to_end = jnp.logical_or(target == 0, target == ep_count - 1)
+        whole_rows = jnp.logical_and(early, jnp.logical_not(to_end))
+        picked_rows = jnp.logical_and(early, to_end)
+
+        @pl.when(early)
+        def _():
+            if d <= 2:
+                landed(tokens.at[source], z_recv.at[source])
+            if 0 in parts:
+                landed(meta_ep.at[source], meta_recv.at[source])
+
+        for c in parts:
+            first, stop = sides[c]
+            if d > 2:
+
+                @pl.when(early)
+                def _():
+                    landed(tokens.at[source, :, first:stop], r_recv.at[source, c])
+
+            def rows_copy(c=c, first=first, stop=stop):
+                spot = tokens.at[source, :, first:stop]
+                return remote(
+                    spot, spot, r_send.at[source, c], r_recv.at[source, c], {"ep": target}
+                )
+
+            def slots_copy(c=c, first=first, stop=stop):
+                return remote(
+                    onward.at[d - 1, :, :, first:stop],
+                    arrived.at[:, t, source, :, first:stop],
+                    r_send.at[source, c],
+                    r_recv.at[source, c],
+                    {"ep": target},
+                )
+
+            send_if(whole_rows, rows_copy)
+
+            @pl.when(picked_rows)
+            def _():
+                def put(columns, value):
+                    onward[d - 1, :, :, columns] = value
+
+                pick_into(source, target, put, first, stop)
+
+            send_if(picked_rows, slots_copy)
+
+    def pick_here(d):
+        source = source_of(d)
+
+        def put(columns, value):
+            arrived[:, t, source, :, columns] = value
+
+        pick_into(source, e, put)
+
     def come(d):
         source = source_of(d)
         spot = arrived.at[:, t, source]
         if direct:
             landed(spot, z_recv.at[source])
+        elif d == 1:
+
+            @pl.when(late)
+            def _():
+                landed(tokens.at[source], z_recv.at[source])
+                landed(meta_ep.at[source], meta_recv.at[source])
+
+            pick_here(d)
         else:
-            landed(tokens.at[source], z_recv.at[source])
-            above = source > e
-            send_if(
-                jnp.logical_or(
-                    jnp.logical_and(above, e > 0),
-                    jnp.logical_and(jnp.logical_not(above), e < ep_count - 1),
-                ),
-                lambda: remote(
-                    tokens.at[source],
-                    tokens.at[source],
-                    z_send.at[source],
-                    z_recv.at[source],
-                    {"ep": jnp.where(source > e, e - 1, e + 1)},
-                ),
-            )
-            landed(meta_ep.at[source], meta_recv.at[source])
-            picked, ignored_weight = picks_of(meta_ep[source], e)
-            picked = picked.astype(bf16)
-
-            def pick_step(columns):
-                part = jnp.dot(picked, tokens[source, :, columns], preferred_element_type=f32)
-                arrived[:, t, source, :, columns] = part.reshape(
-                    local_count, capacity, tile
-                ).astype(bf16)
-
-            tiles(pick_step)
+
+            @pl.when(late)
+            def _():
+                for c, (first, stop) in enumerate(sides):
+                    landed(spot.at[:, :, first:stop], r_recv.at[source, c])
+                landed(meta_ep.at[source], meta_recv.at[source])
+
+            @pl.when(early)
+            def _():
+                pick_here(d)
+
         spread(spot, d)
+
+    def send_keys():
+        for d in range(1, ep_count):
+            there = lax.rem(e + d, ep_count)
+            send(kv_all.at[e], kv_all.at[e], kv_send.at[d], kv_recv.at[e], {"ep": there})
 
     def attend(h):
         def step(b, carried):
@@ -454,42 +556,49 @@
 
         lax.fori_loop(0, model_width // tile, step, 0)
 
+    def begin(row):
+        both_parts = jnp.dot(normed_all[row], shared_both[...], preferred_element_type=f32)
+        gate_part = both_parts[:, :shared_width]
+        up_part = both_parts[:, shared_width:]
+        hidden[row] = (gate_part / (1.0 + jnp.exp(-gate_part)) * up_part).astype(bf16)
+        picked, weight = picks_of(meta_tp[row], e)
+        for n, part in enumerate(split(weight)):
+            weights_here[row, n] = part
+        picked = picked.astype(bf16)
+
+        def columns_step(columns):
+            part = jnp.dot(picked, normed_all[row, :, columns], preferred_element_type=f32)
+            arrived[:, row, e, :, columns] = part.reshape(local_count, capacity, tile).astype(
+                bf16
+            )
+
+        tiles(columns_step)
+
+    def begin_pair(which):
+        def step(n, ignored):
+            begin(which * 2 + n)
+            return ignored
+
+        lax.fori_loop(0, 2, step, 0)
+
     def share():
         def step(row, ignored):
-            both_parts = jnp.dot(normed_all[row], shared_both[...], preferred_element_type=f32)
-            gate_part = both_parts[:, :shared_width]
-            up_part = both_parts[:, shared_width:]
-            hidden = (gate_part / (1.0 + jnp.exp(-gate_part)) * up_part).astype(bf16)
-            ignored_pick, weight = picks_of(meta_tp[row], e)
-            weights = split(weight)
-
             def columns_step(columns):
                 results = routed[:, row, e, :, columns]
                 if capacity % 16:
                     results = results.astype(f32)
                 results = results.reshape(near_count, tile).astype(bf16)
-                part = jnp.dot(hidden, shared_down[:, columns], preferred_element_type=f32)
-                for one in weights:
+                part = jnp.dot(
+                    hidden[row], shared_down[:, columns], preferred_element_type=f32
+                )
+                for n in range(2):
                     part = part + lax.dot_general(
-                        one, results, (((0,), (0,)), ((), ())), preferred_element_type=f32
+                        weights_here[row, n],
+                        results,
+                        (((0,), (0,)), ((), ())),
+                        preferred_element_type=f32,
                     )
                 shared[row, :, columns] = part.astype(bf16)
-
-            tiles(columns_step)
-            return ignored
-
-        lax.fori_loop(0, tp_count, step, 0)
-
-    def pick_own():
-        def step(row, ignored):
-            picked, ignored_weight = picks_of(meta_tp[row], e)
-            picked = picked.astype(bf16)
-
-            def columns_step(columns):
-                part = jnp.dot(picked, normed_all[row, :, columns], preferred_element_type=f32)
-                arrived[:, row, e, :, columns] = part.reshape(
-                    local_count, capacity, tile
-                ).astype(bf16)
 
             tiles(columns_step)
             return ignored
@@ -569,7 +678,8 @@
         part, paired, out, into = item(d)
         for k in range(1, half):
             other = lax.rem(pair + k, half)
-            out(k)[...] = both(d, k).astype(bf16)
+            if state["start"]:
+                out(k)[...] = both(d, k).astype(bf16)
             send(
                 out(k),
                 into(k),
@@ -580,33 +690,44 @@
 
     def finish(d):
         part, paired, out, into = item(d)
-        total = both(d, 0)
-        for k in range(1, half):
-            spot = into(k)
-            landed(spot, back_x_recv.at[d, k])
-            total = total + spot[...].astype(f32)
-        if d < ep_count:
+        if state["start"]:
+            total = both(d, 0)
+            for k in range(1, half):
+                spot = into(k)
+                landed(spot, back_x_recv.at[d, k])
+                total = total + spot[...].astype(f32)
+            if d > ep_count:
+                mixed_sum[...] = total.astype(bf16)
+                return
             routed_done[d] = total.astype(bf16)
+        send(
+            routed_done.at[d],
+            returned.at[e],
+            back_z_send.at[d],
+            back_z_recv.at[e],
+            {"ep": source_of(d)},
+        )
+
+    def lend(d):
+        home = source_of(d)
+        side = jnp.where(home > e, 0, 1)
+        for k in range(half):
+            if state["start"]:
+                lent_out[k] = both(d, k).astype(bf16)
             send(
-                routed_done.at[d],
-                returned.at[e],
-                back_z_send.at[d],
-                back_z_recv.at[e],
-                {"ep": source_of(d)},
-            )
-        elif d == ep_count:
-            channel_out[...] = (total + combined[...]).astype(bf16)
-        else:
-            mixed_sum[...] = total.astype(bf16)
-
-    def combine(d):
-        source = source_of(d)
-        landed(returned.at[source], back_z_recv.at[source])
-        ignored_pick, weight = picks_of(meta_tp[t], source)
+                lent_out.at[k],
+                lent_in.at[side, k],
+                lent_send.at[k],
+                lent_recv.at[side, k],
+                {"ep": home},
+            )
+
+    def add_results(results_of, meta, rank, target=None):
+        ignored_pick, weight = picks_of(meta, rank)
         weights = split(weight)
 
         def columns_step(columns):
-            results = returned[source, :, :, columns]
+            results = results_of(columns)
             if capacity % 16:
                 results = results.astype(f32)
             results = results.reshape(near_count, tile).astype(bf16)
@@ -616,9 +737,57 @@
                 )
                 for one in weights
             )
-            combined[:, columns] = part if d == 1 else combined[:, columns] + part
+            total = combined[:, columns] + part
+            if target is None:
+                combined[:, columns] = total
+            else:
+                target[:, columns] = total.astype(bf16)
 
         tiles(columns_step)
+
+    def gather(k):
+        combined[...] = both(ep_count, k)
+        row = lax.rem(pair + k, half) * 2 + core
+        below = jnp.logical_and(e > 0, first_of(e - 1) == e)
+        above = jnp.logical_and(e < ep_count - 1, first_of(e + 1) == e)
+        for side, there, rank in ((0, below, e - 1), (1, above, e + 1)):
+
+            @pl.when(there)
+            def _():
+                landed(lent_in.at[side, k], lent_recv.at[side, k])
+                add_results(
+                    lambda columns: lent_in[side, k, :, :, columns], meta_tp[row], rank
+                )
+
+    def share_across():
+        part, paired, out, into = item(ep_count)
+        for k in range(1, half):
+            gather(k)
+            out(k)[...] = combined[...].astype(bf16)
+            send(
+                out(k),
+                into(k),
+                back_x_send.at[ep_count, k],
+                back_x_recv.at[ep_count, k],
+                {"tp": lax.rem(pair + k, half) * 2 + core},
+            )
+        gather(0)
+
+    def share_finish():
+        part, paired, out, into = item(ep_count)
+        for k in range(1, half):
+            landed(into(k), back_x_recv.at[ep_count, k])
+            combined[...] = combined[...] + into(k)[...].astype(f32)
+
+    def combine(d):
+        source = source_of(d)
+        landed(returned.at[source], back_z_recv.at[source])
+        add_results(
+            lambda columns: returned[source, :, :, columns],
+            meta_tp[t],
+            source,
+            channel_out if d == ep_count - 1 else None,
+        )
 
     last = ep_count - 1
     pair_count = query.shape[0] // 2
@@ -628,46 +797,81 @@
         experts(d)
         to_sibling(d)
 
-    def attention():
-        for d in range(1, ep_count):
-            landed(kv_all.at[source_of(d)], kv_recv.at[source_of(d)])
-        for n in range(pair_count):
+    for n in range(8, 14):
+        loads[n].wait()
+    all_here(ep_count + 1, (0,))
+    all_here(ep_count, (0,))
+    begin_pair(pair)
+    pass_on(ep_count + 1)
+    pass_on(ep_count)
+    relay(2)
+    relay(1)
+    come(1)
+    branch(early, lambda: come(2))
+    for k in range(1, half):
+        all_here(ep_count + 1, (k,))
+        all_here(ep_count, (k,))
+        begin_pair(lax.rem(pair + k, half))
+    experts(0)
+    relay(3, (0,))
+    pass_on(1)
+    relay(3, (1,))
+    branch(late, lambda: come(2))
+    note(None, lambda: spread(arrived.at[:, t, source_of(2)], 2))
+    expert_item(1)
+    send_keys()
+    branch(late, lambda: lend(1))
+    branch(early, lambda: across(1))
+    come(3)
+    pass_on(2)
+    expert_item(2)
+
+    def out_part():
+        for n in range(1, pair_count):
             attend_two(n)
         loads[14].wait()
         project()
         to_sibling(ep_count + 1)
 
-    pass_on(ep_count + 1)
-    pass_on(ep_count)
-    come(1)
-    all_here(ep_count + 1)
-    all_here(ep_count)
-    pick_own()
-    for n in range(8, 14):
-        loads[n].wait()
-    experts(0)
+    def third():
+        pass_on(3)
+        expert_item(3)
+        across(3)
+
+    branch(late, lambda: across(2))
+    branch(early, lambda: lend(2))
+    for d in range(1, ep_count):
+        landed(kv_all.at[source_of(d)], kv_recv.at[source_of(d)])
+    attend_two(0)
+    branch(early, lambda: finish(1), out_part, lambda: across(ep_count + 1), third)
+    branch(late, third, lambda: finish(2), out_part, lambda: across(ep_count + 1))
+    note(
+        None,
+        lambda: pass_on(3),
+        lambda: to_sibling(3),
+        lambda: across(3),
+        lambda: to_sibling(ep_count + 1),
+        lambda: across(ep_count + 1),
+    )
+    note(late, lambda: lend(1), lambda: across(2), lambda: finish(2))
+    note(early, lambda: lend(2), lambda: across(1), lambda: finish(1))
+    for d in range(4, ep_count):
+        relay(d)
+        come(d)
+        pass_on(d)
+        expert_item(d)
+        across(d)
     share()
     to_sibling(ep_count)
-    for d in range(2, ep_count):
-        come(d)
-        pass_on(d - 1)
-        expert_item(d - 1)
-        across(d - 1)
-        if d == 2:
-            attention()
-        if d > 2:
-            finish(d - 2)
-    pass_on(last)
-    expert_item(last)
-    across(last)
-    across(ep_count + 1)
-    across(ep_count)
-    for d in range(max(1, last - 1), ep_count):
+    for d in range(3, ep_count):
         finish(d)
+    share_across()
     finish(ep_count + 1)
-    for d in range(1, ep_count):
+    share_finish()
+    for d in (1, 2):
+        pl.when(first_of(source_of(d)) != e)(functools.partial(combine, d))
+    for d in range(3, ep_count):
         combine(d)
-    finish(ep_count)
     for wanted, wait in sends:
         if wanted is None:
             wait()
@@ -736,8 +940,13 @@
             room(*spread_block),
             room(tp_count, *token_block),
             room(tp_count, *mixed),
+            room(tp_count, tok_count, shared_down.shape[0]),
+            room(tp_count, 2, local_count * capacity, tok_count),
             wide_room(*token_block),
             room(ep_count, *block),
+            room(*((1 if direct else ep_count - 1,) + block)),
+            room(half, *block),
+            room(2, half, *block),
             room(ep_count, half, *block),
             room(ep_count, half - 1, *block),
             room(ep_count, half - 1, *block),
@@ -753,6 +962,10 @@
             dma((ep_count,)),
             dma((ep_count,)),
             dma((ep_count,)),
+            dma((half,)),
+            dma((2, half)),
+            dma((ep_count, 2)),
+            dma((ep_count, 2)),
             dma((ep_count + 1,)),
             dma((ep_count,)),
             dma((half, ep_count + 2)),
@@ -770,6 +983,38 @@
             collective_id=0, has_side_effects=True, vmem_limit_bytes=67043328
         ),
     )(*small, *weights)
+
+
+def settle_kernel(*refs):
+    count = (len(refs) - 1) // 3
+    sources, targets, rooms = (refs[n * count : (n + 1) * count] for n in range(3))
+    sem = refs[-1]
+    moves = []
+    for n, (source, room, target) in enumerate(zip(sources, rooms, targets)):
+        rows = source.shape[0] // 2
+        for c in range(2):
+            part = pl.ds(c * rows, rows)
+            taken = pltpu.make_async_copy(source.at[part], room.at[part], sem.at[0, n, c])
+            given = pltpu.make_async_copy(room.at[part], target.at[part], sem.at[1, n, c])
+            taken.start()
+            moves.append((taken, given))
+    for taken, given in moves:
+        taken.wait()
+        given.start()
+    for taken, given in moves:
+        given.wait()
+
+
+def settle(*arrays):
+    anywhere = pl.BlockSpec(memory_space=pl.ANY)
+    return pl.pallas_call(
+        settle_kernel,
+        out_shape=tuple(jax.ShapeDtypeStruct(a.shape, a.dtype) for a in arrays),
+        in_specs=[anywhere] * len(arrays),
+        out_specs=(anywhere,) * len(arrays),
+        scratch_shapes=[pltpu.VMEM(a.shape, a.dtype) for a in arrays]
+        + [pltpu.SemaphoreType.DMA((2, len(arrays), 2))],
+    )(*arrays)
 
 
 def body(
@@ -812,7 +1057,7 @@
             shared_down,
         ),
     )
-    return (mixer_out, channel_out)
+    return settle(mixer_out, channel_out)
 
 
 def solution(mesh):

time: 117 us -> 95.3 us (0.81)
  Pallas kernels: 112 us -> 94.5 us
  local copies, waits for them, and re-layouts: 3.65 us -> 0 us
    pallas_call x1, Pallas kernels: 112 us -> 92.4 us  [whole(): pl.pallas_call(functools.partial(whole_kernel, ep_count, tp_count, direct...]
    unnamed x2 -> x0, local copies, waits for them, and re-layouts: 3.65 us -> none
    pallas_call x0 -> x1, Pallas kernels: none -> 2.01 us  [settle(): pl.pallas_call(settle_kernel, out_shape=tuple((jax.ShapeDtypeStruct(a.sha...]
where the time goes in v2:
time: 95.3 us; the launch traced here: 95.1 us
  Pallas kernels  94.5 us (99%)
    pallas_call x1, Pallas kernels, whole(): pl.pallas_call(functools.partial(whole_kernel, ep_count, tp_count, direct...  92.4 us
    pallas_call x1, Pallas kernels, settle(): pl.pallas_call(settle_kernel, out_shape=tuple((jax.ShapeDtypeStruct(a.sha...  2.01 us

profile of v2, /device:TPU:0, one launch (start us, length us, event | category | flops | bytes accessed | tf_op | source)
XLA Modules:
  0.0 95.1 jit_solution(2723417580971585694)
XLA Ops:
  0.6 92.4 %shard_map.158 = (bf16[128,2048]{1,0:T(8,128)(2,1)}, bf16[96,2048]{1,0:T(8,128)(2,1)}) custom-call(bf16[384,256]{1,0:T(8,128)(2,1)} %queries_hbm.1, bf16[384,128]{1,0:T(8,128)(2,1)} %kv_hbm.1, f32[1,64]{1,0:T(1,128)} %bitcast.8, f32[1,64]{1,0:T(1,128)} %bitcast.9, bf16[128,2048]{1,0:T(8,128)(2,1)} %batch_hbm.1, f32[1,2048]{1,0:T(1,128)} %bitcast.5, ...), custom_call_target="tpu_custom_call" | custom-call | tf_op jit(solution)/shard_map/pallas_call | solution.py:909
  93.1 2.0 %shard_map.159 = (bf16[96,2048]{1,0:T(8,128)(2,1)}, bf16[128,2048]{1,0:T(8,128)(2,1)}) custom-call(bf16[96,2048]{1,0:T(8,128)(2,1)} %get-tuple-element.4.refs_0_, bf16[128,2048]{1,0:T(8,128)(2,1)} %get-tuple-element.5.refs_1_), custom_call_target="tpu_custom_call" | custom-call | tf_op jit(solution)/shard_map/pallas_call | solution.py:1010

commit v3 on v2

--- a/solution.py
+++ b/solution.py
@@ -711,7 +711,7 @@
     def lend(d):
         home = source_of(d)
         side = jnp.where(home > e, 0, 1)
-        for k in range(half):
+        for k in list(range(1, half)) + [0]:
             if state["start"]:
                 lent_out[k] = both(d, k).astype(bf16)
             send(
@@ -722,7 +722,7 @@
                 {"ep": home},
             )
 
-    def add_results(results_of, meta, rank, target=None):
+    def add_results(results_of, meta, rank):
         ignored_pick, weight = picks_of(meta, rank)
         weights = split(weight)
 
@@ -737,11 +737,7 @@
                 )
                 for one in weights
             )
-            total = combined[:, columns] + part
-            if target is None:
-                combined[:, columns] = total
-            else:
-                target[:, columns] = total.astype(bf16)
+            combined[:, columns] = combined[:, columns] + part
 
         tiles(columns_step)
 
@@ -775,9 +771,11 @@
 
     def share_finish():
         part, paired, out, into = item(ep_count)
+        total = combined[...]
         for k in range(1, half):
             landed(into(k), back_x_recv.at[ep_count, k])
-            combined[...] = combined[...] + into(k)[...].astype(f32)
+            total = total + into(k)[...].astype(f32)
+        channel_out[...] = total.astype(bf16)
 
     def combine(d):
         source = source_of(d)
@@ -786,7 +784,6 @@
             lambda columns: returned[source, :, :, columns],
             meta_tp[t],
             source,
-            channel_out if d == ep_count - 1 else None,
         )
 
     last = ep_count - 1
@@ -819,59 +816,49 @@
     branch(late, lambda: come(2))
     note(None, lambda: spread(arrived.at[:, t, source_of(2)], 2))
     expert_item(1)
-    send_keys()
-    branch(late, lambda: lend(1))
+    branch(late, send_keys, lambda: lend(1))
     branch(early, lambda: across(1))
     come(3)
+    branch(early, send_keys)
+    note(None, send_keys)
     pass_on(2)
     expert_item(2)
 
-    def out_part():
-        for n in range(1, pair_count):
-            attend_two(n)
-        loads[14].wait()
-        project()
-        to_sibling(ep_count + 1)
-
-    def third():
-        pass_on(3)
-        expert_item(3)
-        across(3)
-
     branch(late, lambda: across(2))
-    branch(early, lambda: lend(2))
+    branch(early, lambda: lend(2), lambda: finish(1))
     for d in range(1, ep_count):
         landed(kv_all.at[source_of(d)], kv_recv.at[source_of(d)])
     attend_two(0)
-    branch(early, lambda: finish(1), out_part, lambda: across(ep_count + 1), third)
-    branch(late, third, lambda: finish(2), out_part, lambda: across(ep_count + 1))
-    note(
-        None,
-        lambda: pass_on(3),
-        lambda: to_sibling(3),
-        lambda: across(3),
-        lambda: to_sibling(ep_count + 1),
-        lambda: across(ep_count + 1),
-    )
-    note(late, lambda: lend(1), lambda: across(2), lambda: finish(2))
-    note(early, lambda: lend(2), lambda: across(1), lambda: finish(1))
-    for d in range(4, ep_count):
-        relay(d)
-        come(d)
+    for d in range(3, ep_count):
+        if d > 3:
+            relay(d)
+            come(d)
         pass_on(d)
         expert_item(d)
         across(d)
+    branch(late, lambda: finish(2))
+    note(late, lambda: lend(1), lambda: across(2), lambda: finish(2))
+    note(early, lambda: lend(2), lambda: across(1), lambda: finish(1))
+    for n in range(1, pair_count):
+        attend_two(n)
+    loads[14].wait()
+    project()
+    to_sibling(ep_count + 1)
+    across(ep_count + 1)
+    branch(late, lambda: finish(3))
     share()
     to_sibling(ep_count)
-    for d in range(3, ep_count):
+    branch(early, lambda: finish(3))
+    note(None, lambda: finish(3))
+    for d in range(4, ep_count):
         finish(d)
     share_across()
     finish(ep_count + 1)
-    share_finish()
     for d in (1, 2):
         pl.when(first_of(source_of(d)) != e)(functools.partial(combine, d))
     for d in range(3, ep_count):
         combine(d)
+    share_finish()
     for wanted, wait in sends:
         if wanted is None:
             wait()

time: 95.3 us -> 93.5 us (0.981)
  Pallas kernels: 94.5 us -> 92.7 us
    pallas_call x1, Pallas kernels: 92.4 us -> 90.7 us  [whole(): pl.pallas_call(functools.partial(whole_kernel, ep_count, tp_count, direct...]
where the time goes in v3:
time: 93.5 us; the launch traced here: 93.3 us
  Pallas kernels  92.7 us (99%)
    pallas_call x1, Pallas kernels, whole(): pl.pallas_call(functools.partial(whole_kernel, ep_count, tp_count, direct...  90.7 us
    pallas_call x1, Pallas kernels, settle(): pl.pallas_call(settle_kernel, out_shape=tuple((jax.ShapeDtypeStruct(a.sha...  2.01 us

profile of v3, /device:TPU:0, one launch (start us, length us, event | category | flops | bytes accessed | tf_op | source)
XLA Modules:
  0.0 93.3 jit_solution(2131520800383455862)
XLA Ops:
  0.6 90.7 %shard_map.158 = (bf16[128,2048]{1,0:T(8,128)(2,1)}, bf16[96,2048]{1,0:T(8,128)(2,1)}) custom-call(bf16[384,256]{1,0:T(8,128)(2,1)} %queries_hbm.1, bf16[384,128]{1,0:T(8,128)(2,1)} %kv_hbm.1, f32[1,64]{1,0:T(1,128)} %bitcast.8, f32[1,64]{1,0:T(1,128)} %bitcast.9, bf16[128,2048]{1,0:T(8,128)(2,1)} %batch_hbm.1, f32[1,2048]{1,0:T(1,128)} %bitcast.5, ...), custom_call_target="tpu_custom_call" | custom-call | tf_op jit(solution)/shard_map/pallas_call | solution.py:896
  91.3 2.0 %shard_map.159 = (bf16[96,2048]{1,0:T(8,128)(2,1)}, bf16[128,2048]{1,0:T(8,128)(2,1)}) custom-call(bf16[96,2048]{1,0:T(8,128)(2,1)} %get-tuple-element.4.refs_0_, bf16[128,2048]{1,0:T(8,128)(2,1)} %get-tuple-element.5.refs_1_), custom_call_target="tpu_custom_call" | custom-call | tf_op jit(solution)/shard_map/pallas_call | solution.py:997

commit v4 on v3

--- a/solution.py
+++ b/solution.py
@@ -591,13 +591,12 @@
                 part = jnp.dot(
                     hidden[row], shared_down[:, columns], preferred_element_type=f32
                 )
-                for n in range(2):
-                    part = part + lax.dot_general(
-                        weights_here[row, n],
-                        results,
-                        (((0,), (0,)), ((), ())),
-                        preferred_element_type=f32,
-                    )
+                part = part + lax.dot_general(
+                    weights_here[row].reshape(2 * near_count, tok_count),
+                    jnp.concatenate([results, results], axis=0),
+                    (((0,), (0,)), ((), ())),
+                    preferred_element_type=f32,
+                )
                 shared[row, :, columns] = part.astype(bf16)
 
             tiles(columns_step)
@@ -724,18 +723,18 @@
 
     def add_results(results_of, meta, rank):
         ignored_pick, weight = picks_of(meta, rank)
-        weights = split(weight)
+        weights = jnp.concatenate(split(weight), axis=0)
 
         def columns_step(columns):
             results = results_of(columns)
             if capacity % 16:
                 results = results.astype(f32)
             results = results.reshape(near_count, tile).astype(bf16)
-            part = sum(
-                lax.dot_general(
-                    one, results, (((0,), (0,)), ((), ())), preferred_element_type=f32
-                )
-                for one in weights
+            part = lax.dot_general(
+                weights,
+                jnp.concatenate([results, results], axis=0),
+                (((0,), (0,)), ((), ())),
+                preferred_element_type=f32,
             )
             combined[:, columns] = combined[:, columns] + part
 

time: 93.5 us -> 93.3 us (level)
  no operation moved by 1% of the time
where the time goes in v4:
time: 93.3 us; the launch traced here: 93 us
  Pallas kernels  92.4 us (99%)
    pallas_call x1, Pallas kernels, whole(): pl.pallas_call(functools.partial(whole_kernel, ep_count, tp_count, direct...  90.4 us
    pallas_call x1, Pallas kernels, settle(): pl.pallas_call(settle_kernel, out_shape=tuple((jax.ShapeDtypeStruct(a.sha...  2.01 us

profile of v4, /device:TPU:0, one launch (start us, length us, event | category | flops | bytes accessed | tf_op | source)
XLA Modules:
  0.0 93.0 jit_solution(5606761870869572721)
XLA Ops:
  0.6 90.4 %shard_map.158 = (bf16[128,2048]{1,0:T(8,128)(2,1)}, bf16[96,2048]{1,0:T(8,128)(2,1)}) custom-call(bf16[384,256]{1,0:T(8,128)(2,1)} %queries_hbm.1, bf16[384,128]{1,0:T(8,128)(2,1)} %kv_hbm.1, f32[1,64]{1,0:T(1,128)} %bitcast.8, f32[1,64]{1,0:T(1,128)} %bitcast.9, bf16[128,2048]{1,0:T(8,128)(2,1)} %batch_hbm.1, f32[1,2048]{1,0:T(1,128)} %bitcast.5, ...), custom_call_target="tpu_custom_call" | custom-call | tf_op jit(solution)/shard_map/pallas_call | solution.py:895
  91.0 2.0 %shard_map.159 = (bf16[96,2048]{1,0:T(8,128)(2,1)}, bf16[128,2048]{1,0:T(8,128)(2,1)}) custom-call(bf16[96,2048]{1,0:T(8,128)(2,1)} %get-tuple-element.4.refs_0_, bf16[128,2048]{1,0:T(8,128)(2,1)} %get-tuple-element.5.refs_1_), custom_call_target="tpu_custom_call" | custom-call | tf_op jit(solution)/shard_map/pallas_call | solution.py:996
